TPU v7x, 32 devices: a whole 2x2x4 slice. The times are simulated.
32 devices in a mesh: grp: 2 (over x), fs: 4 (over y, core), tp: 4 (over z).
Axes of the slice: x: 2, y: 2, z: 4, core: 2. Of those that a mesh axis runs over, the one named last changes fastest.
Arguments:
- prompt_tokens: bfloat16 [4096, 2048], P(('grp', 'fs', 'tp')), parts along dimension 0, may hold values from -6 to 6
- up_weight: float32 [2048, 8192], P('fs', 'tp'), may hold values from -0.125 to 0.125
- down_weight: float32 [2048, 8192], P('fs', 'tp'), may hold values from -0.0625 to 0.0625
- pre_gain: float32 [2048], P('fs'), may hold values from 0.1 to 1.9
- post_gain: float32 [2048], replicated, may hold values from 0.1 to 1.9
Outputs:
- mixed: bfloat16 [4096, 2048], P(('grp', 'fs', 'tp')), parts along dimension 0
- sampler_up: bfloat16 [4096, 8192], P('grp', 'tp'), parts along dimension 0
- sampler_down: bfloat16 [4096, 8192], P('grp', 'tp'), parts along dimension 0
There are 2 independent parts, one for each index of `grp`. A program takes and returns all parts, laid end to end along the dimension named above; an argument that names none is the same for every part. Nothing has to cross between parts.
All inputs are finite; a program needn't handle non-finite values.
Results may differ from a plain program's by a relative error of at most 0.015.
Values may be sent and summed in bfloat16 or wider, within the bound.
A program may use at most 128 MiB of HBM per device.

v0:
```python
import jax
import jax.numpy as jnp
from jax import lax
from jax.sharding import PartitionSpec as P


def per_device(prompt_tokens, up_weight, down_weight, pre_gain, post_gain):
    up_local = (up_weight * pre_gain[:, None]).astype(jnp.bfloat16)
    down_local = down_weight.astype(jnp.bfloat16)
    values = prompt_tokens.astype(jnp.float32)
    normed = (values * lax.rsqrt(jnp.mean(values * values, axis=1, keepdims=True) + 1e-06)).astype(
        jnp.bfloat16
    )
    sampler_up, sampler_down = (
        lax.all_gather(up_local, "fs", axis=0, tiled=True),
        lax.all_gather(down_local, "fs", axis=0, tiled=True),
    )
    lifted = jnp.dot(
        lax.all_gather(normed, "tp", axis=0, tiled=True),
        sampler_up,
        preferred_element_type=jnp.float32,
    )
    hidden = jnp.square(jax.nn.relu(lifted)).astype(jnp.bfloat16)
    summed = lax.psum_scatter(
        lax.dot_general(
            hidden, sampler_down, (((1,), (1,)), ((), ())), preferred_element_type=jnp.float32
        ).astype(jnp.bfloat16),
        "tp",
        scatter_dimension=0,
        tiled=True,
    ).astype(jnp.float32)
    scaled = summed * lax.rsqrt(jnp.mean(summed * summed, axis=1, keepdims=True) + 1e-06)
    mixed = (scaled * post_gain[None, :]).astype(jnp.bfloat16)
    return (mixed, sampler_up, sampler_down)


def solution(mesh):
    placed = (P(("grp", "fs", "tp"), None), P("fs", "tp"), P("fs", "tp"), P("fs"), P())
    return jax.shard_map(
        per_device,
        mesh=mesh,
        in_specs=placed,
        out_specs=(P(("grp", "fs", "tp"), None), P("grp", "tp"), P("grp", "tp")),
        check_vma=False,
    )
```

profile of v0, /device:TPU:0, one launch (start us, length us, event | category | flops | bytes accessed | tf_op | source)
XLA Modules:
  0.0 265.7 jit_solution(5066965389178030191)
XLA Ops:
  7.2 0.0 all-gather.4.cloned.1.call-start
  7.2 1.2 fusion
  8.4 2.0 fusion.1
  10.4 0.0 all-gather.4.cloned.1.call-update
  10.5 0.0 all-gather.6.cloned.1.call-start
  10.5 3.8 %multiply_convert_fusion.1 = bf16[512,2048]{1,0:T(8,128)(2,1)} fusion(f32[512,2048]{1,0:T(8,128)} %param.6, f32[512]{0:T(512)} %param.8), kind=kLoop, calls=%fused_computation.1 | loop fusion | flops 2097152 | bytes 6293504 | tf_op jit(solution)/shard_map/convert_element_type | solution.py:8
  14.3 0.0 all-gather.6.cloned.1.call-update
  14.3 0.0 all-gather.8.cloned.1.call-start
  14.4 3.8 %convert_element_type.28 = bf16[512,2048]{1,0:T(8,128)(2,1)} convert(f32[512,2048]{1,0:T(8,128)} %param.7) | non-fusion elementwise | flops 1048576 | bytes 6291456 | tf_op jit(solution)/shard_map/convert_element_type | solution.py:9
  18.2 0.0 all-gather.8.cloned.1.call-update
  18.2 0.0 copy-start
  18.3 0.0 reduce-scatter.2.cloned.1.call-start
  18.3 40.7 %all-gather.4.cloned.1.call-done = bf16[512,2048]{1,0:T(8,128)(2,1)} async-done(((bf16[128,2048]{1,0:T(8,128)(2,1)}), bf16[512,2048]{1,0:T(8,128)(2,1)}) %all-gather.4.cloned.1.call-update) | async-done | bytes 2097168 | tf_op jit(solution)/shard_map/all_gather | solution.py:19
  59.0 59.2 %all-gather.6.cloned.1.call-done = bf16[2048,2048]{1,0:T(8,128)(2,1)} async-done(((bf16[512,2048]{1,0:T(8,128)(2,1)}), bf16[2048,2048]{1,0:T(8,128)(2,1)}) %all-gather.6.cloned.1.call-update) | async-done | bytes 8388624 | tf_op jit(solution)/shard_map/all_gather | solution.py:15
  118.2 60.4 %all-gather.8.cloned.1.call-done = bf16[2048,2048]{1,0:T(8,128)(2,1)} async-done(((bf16[512,2048]{1,0:T(8,128)(2,1)}), bf16[2048,2048]{1,0:T(8,128)(2,1)}) %all-gather.8.cloned.1.call-update) | async-done | bytes 8388624 | tf_op jit(solution)/shard_map/all_gather | solution.py:16
  178.7 16.5 %convolution_convert_fusion = bf16[512,2048]{1,0:T(8,128)(2,1)} fusion(bf16[2048,2048]{1,0:T(8,128)(2,1)} %all-gather.8.cloned.1.call-done, bf16[512,2048]{1,0:T(8,128)(2,1)} %all-gather.4.cloned.1.call-done, bf16[2048,2048]{1,0:T(8,128)(2,1)} %all-gather.6.cloned.1.call-done), kind=kOutput, calls=%fused_computation.2 | convolution fusion | flops 8594128896 | bytes 20971520 | tf_op jit(solution)/shard_map/dot_general | solution.py:25
  195.2 0.0 reduce-scatter.2.cloned.1.call-update
  195.2 43.8 %reduce-scatter.2.cloned.1.call-done = bf16[128,2048]{1,0:T(8,128)(2,1)} async-done(((bf16[512,2048]{1,0:T(8,128)(2,1)}), bf16[128,2048]{1,0:T(8,128)(2,1)}) %reduce-scatter.2.cloned.1.call-update) | async-done | bytes 524304 | tf_op jit(solution)/shard_map/reduce_scatter | solution.py:24
  239.0 1.2 fusion.2
  240.2 0.0 copy-done
  240.2 2.0 fusion.4
  242.3 8.4 %copy.10 = bf16[2048,2048]{1,0:T(8,128)(2,1)} copy(bf16[2048,2048]{1,0:T(8,128)(2,1)} %all-gather.6.cloned.1.call-done) | data formatting | bytes 16777216
  250.7 8.4 %copy.11 = bf16[2048,2048]{1,0:T(8,128)(2,1)} copy(bf16[2048,2048]{1,0:T(8,128)(2,1)} %all-gather.8.cloned.1.call-done) | data formatting | bytes 16777216
  (2 shorter events, 0.0 us)
Async XLA Ops:
  7.2 51.8 %all-gather.4.cloned.1.call-start = ((), (), s32[]{:S(2)}) async-start(), calls=%async_computation.1 | async-start | bytes 2621440 | tf_op jit(solution)/shard_map/all_gather | solution.py:19
  10.5 107.8 %all-gather.6.cloned.1.call-start = ((), (), s32[]{:S(2)}) async-start(), calls=%async_computation.2 | async-start | bytes 10485760 | tf_op jit(solution)/shard_map/all_gather | solution.py:15
  14.3 164.3 %all-gather.8.cloned.1.call-start = ((), (), s32[]{:S(2)}) async-start(), calls=%async_computation.3 | async-start | bytes 10485760 | tf_op jit(solution)/shard_map/all_gather | solution.py:16
  18.2 222.0 %copy-start = (f32[2048]{0:T(1024)S(1)}, f32[2048]{0:T(1024)}, u32[]{:S(2)}) copy-start(f32[2048]{0:T(1024)} %param.9) | copy-start | bytes 24580
  18.3 220.7 %reduce-scatter.2.cloned.1.call-start = ((), (), s32[]{:S(2)}) async-start(), calls=%async_computation.4 | async-start | bytes 2621440 | tf_op jit(solution)/shard_map/reduce_scatter | solution.py:24
Sparse Core Ops, SparseCore 0:
  10.6 48.3 all-gather.3
  61.1 57.0 all-gather.5
  120.4 58.2 all-gather.7
  195.3 43.6 reduce-scatter.1
where the time goes:
time: 266 us
  waiting for transfers between devices  204 us (77%)
  local copies, waits for them, and re-layouts  16.9 us (6%)
  matrix products  16.5 us (6%)
  other arithmetic  14.1 us (5%)
  between operations  13.8 us (5%)
    all_gather x1, waiting for transfers between devices, per_device(): lax.all_gather(down_local, 'fs', axis=0, tiled=True)  60.4 us
    all_gather x1, waiting for transfers between devices, per_device(): lax.all_gather(up_local, 'fs', axis=0, tiled=True)  59.2 us
    reduce_scatter x1, waiting for transfers between devices, per_device(): lax.psum_scatter(lax.dot_general(hidden, sampler_down, (((1,), (1,)), (()...  43.8 us
    all_gather x1, waiting for transfers between devices, per_device(): lax.all_gather(normed, 'tp', axis=0, tiled=True)  40.7 us
    unnamed x4, local copies, waits for them, and re-layouts  16.9 us
    dot_general x1, matrix products, per_device(): lax.dot_general(hidden, sampler_down, (((1,), (1,)), ((), ())), preferred...  16.5 us
  transfers between devices with their start and end apart: 4, of which 4 were waited for; matrix products, arithmetic and copies ran while one was open for 3% of the time, Pallas kernels for 0%

commit v1 on v0

v1 whole, which is shorter than its diff:
```python
import functools

import jax
import jax.numpy as jnp
from jax import lax
from jax.experimental import pallas as pl
from jax.experimental.pallas import tpu as pltpu
from jax.sharding import PartitionSpec as P

MESH = pl.DeviceIdType.MESH
BF16 = jnp.bfloat16
F32 = jnp.float32


def layer_kernel(sizes, tok_ref, gain_ref, post_ref, up_hbm, down_hbm, mixed_ref, up_full, down_full,
                 stage, tok, hidden, rbuf, sbuf, total,
                 load_sem, tsend, trecv, ysend, yrecv, xsend, xrecv, csend, crecv, osend, orecv, rsend, rrecv):
    G, F, T, NC = sizes
    Y = F // 2
    g, fs, z = lax.axis_index("grp"), lax.axis_index("fs"), lax.axis_index("tp")
    y, c = fs // 2, fs % 2
    R, H = up_hbm.shape
    piece = R // G
    CR = piece // NC
    rows_t = tok_ref.shape[0]
    full = (up_full, down_full)
    hbm = (up_hbm, down_hbm)
    partner = y * 2 + (1 - c)
    not_first, not_last = z > 0, z < T - 1

    def loads(m, e):
        r = pl.ds(pl.multiple_of(((g + e) % G) * piece, piece), piece)
        return pltpu.make_async_copy(hbm[m].at[r], stage.at[m, r], load_sem.at[m, e])

    for m in range(2):
        for e in range(G):
            loads(m, e).start()

    barrier = pltpu.get_barrier_semaphore()
    for d in range(1, Y):
        pl.semaphore_signal(barrier, inc=1, device_id={"fs": ((y + d) % Y) * 2 + c}, device_id_type=MESH)
    for e in range(1, G):
        pl.semaphore_signal(barrier, inc=1, device_id={"grp": (g + e) % G}, device_id_type=MESH)
    pl.semaphore_signal(barrier, inc=1, device_id={"fs": partner}, device_id_type=MESH)

    @pl.when(not_first)
    def _():
        pl.semaphore_signal(barrier, inc=1, device_id={"tp": z - 1}, device_id_type=MESH)

    @pl.when(not_last)
    def _():
        pl.semaphore_signal(barrier, inc=1, device_id={"tp": z + 1}, device_id_type=MESH)

    values = tok_ref[...].astype(F32)
    scale = lax.rsqrt(jnp.mean(values * values, axis=1, keepdims=True) + 1e-06)
    tok[z] = (values * scale).astype(BF16)

    def convert(m, start, n):
        for i in range(0, n, CR):
            r = pl.ds(pl.multiple_of(start + i, CR), CR)
            v = stage[m, r, :]
            if m == 0:
                v = v * gain_ref[r, :]
            full[m][pl.ds(pl.multiple_of(fs * R + start + i, CR), CR), :] = v.astype(BF16)

    def remote(ref, rows, ss, rs, dev):
        return pltpu.make_async_remote_copy(ref.at[rows], ref.at[rows], ss, rs, device_id=dev, device_id_type=MESH)

    def chunk_rows(shard, e, q):
        return pl.ds(pl.multiple_of(shard * R + ((g + e) % G) * piece + q * CR, CR), CR)

    def y_copy(m, d, q):
        return remote(full[m], chunk_rows(fs, 0, q), ysend.at[m, d, q], yrecv.at[m, d, q],
                      {"fs": ((y + d) % Y) * 2 + c})

    def y_in(m, d, q):
        shard = ((y - d + Y) % Y) * 2 + c
        return remote(full[m], chunk_rows(shard, 0, q), ysend.at[m, d, q], yrecv.at[m, d, q], {"fs": partner})

    def x_copy(m, d, q, e):
        shard = ((y - d + Y) % Y) * 2 + c
        return remote(full[m], chunk_rows(shard, 0, q), xsend.at[m, d, q, e], xrecv.at[m, d, q, e],
                      {"grp": (g + e) % G})

    def x_in(m, d, q, e):
        shard = ((y - d + Y) % Y) * 2 + c
        return remote(full[m], chunk_rows(shard, G - e, q), xsend.at[m, d, q, e], xrecv.at[m, d, q, e],
                      {"grp": (g + e) % G})

    def c_copy(m, d, q, e):
        shard = ((y - d + Y) % Y) * 2 + c
        return remote(full[m], chunk_rows(shard, (G - e) % G, q), csend.at[m, d, q, e], crecv.at[m, d, q, e],
                      {"fs": partner})

    def c_in(m, d, q, e):
        shard = ((y - d + Y) % Y) * 2 + (1 - c)
        return remote(full[m], chunk_rows(shard, (G - e) % G, q), csend.at[m, d, q, e], crecv.at[m, d, q, e],
                      {"fs": partner})

    def own_copy(m, sign):
        shard = fs if sign else partner
        r = pl.ds(pl.multiple_of(shard * R, R), R)
        return remote(full[m], r, osend.at[m], orecv.at[m], {"fs": partner})

    pl.semaphore_wait(barrier, (Y - 1) + (G - 1) + 1 + not_first.astype(jnp.int32) + not_last.astype(jnp.int32))

    def tok_out(dirn, k):
        b = z - k if dirn == 0 else z + k
        dev = z + 1 if dirn == 0 else z - 1
        return pltpu.make_async_remote_copy(tok.at[b], tok.at[b], tsend.at[dirn, k], trecv.at[dirn, k],
                                            device_id={"tp": dev}, device_id_type=MESH)

    def tok_in(dirn, k):
        b = z - k - 1 if dirn == 0 else z + k + 1
        dev = z + 1 if dirn == 0 else z - 1
        return pltpu.make_async_remote_copy(tok.at[b], tok.at[b], tsend.at[dirn, k], trecv.at[dirn, k],
                                            device_id={"tp": dev}, device_id_type=MESH)

    def has_out(dirn, k):
        return (z - k >= 0) & not_last if dirn == 0 else (z + k <= T - 1) & not_first

    def has_in(dirn, k):
        return z - k - 1 >= 0 if dirn == 0 else z + k + 1 <= T - 1

    def tok_step(k):
        for dirn in range(2):
            if k > 0:
                @pl.when(has_in(dirn, k - 1))
                def _():
                    tok_in(dirn, k - 1).wait_recv()
            if k < T - 1:
                @pl.when(has_out(dirn, k))
                def _():
                    tok_out(dirn, k).start()

    tok_step(0)

    for m in range(2):
        loads(m, 0).wait()
        for q in range(NC):
            convert(m, pl.multiple_of(g * piece, piece) + q * CR, CR)
            for d in range(1, Y):
                y_copy(m, d, q).start()
        for e in range(1, G):
            loads(m, e).wait()
            convert(m, pl.multiple_of(((g + e) % G) * piece, piece), piece)
        own_copy(m, True).start()

    def fwd(m, q):
        for d in range(1, Y):
            if q < NC:
                y_in(m, d, q).wait_recv()
                for e in range(1, G):
                    x_copy(m, d, q, e).start()
                c_copy(m, d, q, 0).start()
            if q >= LAG:
                for e in range(1, G):
                    x_in(m, d, q - LAG, e).wait_recv()
                    c_copy(m, d, q - LAG, e).start()

    LAG = 2
    steps = NC + LAG
    tok_at = {max(1, (steps * k) // (T - 1)): k for k in range(1, T - 1)}
    for q in range(steps):
        fwd(0, q)
        if q in tok_at:
            tok_step(tok_at[q])
    for k in range(1, T - 1):
        if k not in tok_at.values():
            tok_step(k)
    own_copy(0, False).wait_recv()
    for d in range(1, Y):
        for q in range(NC):
            for e in range(G):
                c_in(0, d, q, e).wait_recv()

    NT = min(512, H)

    def first_mm(t):
        x = tok[t]
        @pl.loop(0, H // NT)
        def _(j):
            cols = pl.ds(pl.multiple_of(j * NT, NT), NT)
            l = jnp.maximum(jnp.dot(x, up_full[:, cols], preferred_element_type=F32), 0.0)
            hidden[t, :, cols] = (l * l).astype(BF16)

    def second_mm(t, f):
        w = down_full[pl.ds(pl.multiple_of(f * R, R), R), :]
        return lax.dot_general(hidden[t], w, (((1,), (1,)), ((), ())), preferred_element_type=F32).astype(BF16)

    side = jnp.minimum(z, T - 1 - z)

    def order(k):
        n = T - 1 - k
        near = jnp.where(n % 2 == 1, z + (n + 1) // 2, z - n // 2)
        far = jnp.where(z < T - 1 - z, z + (n - side), z - (n - side))
        return jnp.where(n <= 2 * side, near, far)

    def rs_copy(t, f, right):
        dev = z + 1 if right else z - 1
        slot = t if right else jnp.where(t == z - 1, T, t)
        return pltpu.make_async_remote_copy(sbuf.at[t, f], rbuf.at[slot, f], rsend.at[t, f], rrecv.at[slot, f],
                                            device_id={"tp": dev}, device_id_type=MESH)

    def rs_in(slot, f):
        return pltpu.make_async_remote_copy(sbuf.at[0, f], rbuf.at[slot, f], rsend.at[0, f], rrecv.at[slot, f],
                                            device_id={"tp": z}, device_id_type=MESH)

    def unit(t, f):
        p = second_mm(t, f)
        inner = ((t > z) & not_first) | ((t < z) & not_last)

        @pl.when(inner)
        def _():
            rs_in(t, f).wait_recv()
            sbuf[t, f] = (p.astype(F32) + rbuf[t, f].astype(F32)).astype(BF16)

        @pl.when(jnp.logical_not(inner))
        def _():
            sbuf[t, f] = p

        @pl.when(t > z)
        def _():
            rs_copy(t, f, True).start()

        @pl.when(t < z)
        def _():
            rs_copy(t, f, False).start()

    def feature(d, other):
        return ((y - d + Y) % Y) * 2 + (1 - c if other else c)

    def own_unit(f):
        cols = pl.ds(pl.multiple_of(f * R, R), R)
        total[:, cols] = second_mm(z, f).astype(F32)

    own_copy(1, False).wait_recv()
    todo = list(range(steps))

    def some(n):
        for _ in range(n):
            if todo:
                fwd(1, todo.pop(0))

    for k in range(T):
        t = order(k) if k < T - 1 else z
        if k == 0:
            tok_step(T - 1)
        first_mm(t)
        some(1)
        for other in range(2):
            if k < T - 1:
                unit(t, feature(0, other))
            else:
                own_unit(feature(0, other))
            some(1)
    some(len(todo))
    for d in range(1, Y):
        for q in range(NC):
            for e in range(G):
                c_in(1, d, q, e).wait_recv()
    for d in range(1, Y):
        for other in range(2):
            f = feature(d, other)
            for k in range(T - 1):
                unit(order(k), f)
            own_unit(f)

    for f in range(F):
        cols = pl.ds(f * R, R)

        @pl.when(not_first)
        def _():
            rs_in(z, f).wait_recv()
            total[:, cols] += rbuf[z, f].astype(F32)

        @pl.when(not_last)
        def _():
            rs_in(T, f).wait_recv()
            total[:, cols] += rbuf[T, f].astype(F32)

    s = total[...]
    inv = lax.rsqrt(jnp.mean(s * s, axis=1, keepdims=True) + 1e-06)
    mixed_ref[...] = (s * inv * post_ref[...]).astype(BF16)

    for k in range(T - 1):
        for dirn in range(2):
            @pl.when(has_out(dirn, k))
            def _():
                tok_out(dirn, k).wait_send()
    for m in range(2):
        own_copy(m, True).wait_send()
        for d in range(1, Y):
            for q in range(NC):
                y_copy(m, d, q).wait_send()
                for e in range(G):
                    if e:
                        x_copy(m, d, q, e).wait_send()
                    c_copy(m, d, q, e).wait_send()
    for k in range(T - 1):
        t = order(k)
        for f in range(F):
            rs_copy(t, f, True).wait_send()


def out_kernel(up_v, down_v, up_o, down_o, sem):
    n = sem.shape[1]
    r = up_v.shape[0] // n
    cps = [pltpu.make_async_copy(a.at[pl.ds(i * r, r)], b.at[pl.ds(i * r, r)], sem.at[m, i])
           for m, (a, b) in enumerate(((up_v, up_o), (down_v, down_o))) for i in range(n)]
    for cp in cps:
        cp.start()
    for cp in cps:
        cp.wait()


def solution(mesh):
    G, F, T = mesh.shape["grp"], mesh.shape["fs"], mesh.shape["tp"]
    Y = F // 2

    def per_device(prompt_tokens, up_weight, down_weight, pre_gain, post_gain):
        rows, D = prompt_tokens.shape
        R, H = up_weight.shape
        piece = R // G
        CR = max(16, piece // 8)
        NC = piece // CR
        DMA = pltpu.SemaphoreType.DMA
        vm, any_ = pl.BlockSpec(memory_space=pltpu.VMEM), pl.BlockSpec(memory_space=pl.ANY)
        mixed, up, down = pl.pallas_call(
            functools.partial(layer_kernel, (G, F, T, NC)),
            out_shape=(jax.ShapeDtypeStruct((rows, D), BF16),
                       pltpu.VMEM((F * R, H), BF16), pltpu.VMEM((F * R, H), BF16)),
            in_specs=[vm, vm, vm, any_, any_],
            out_specs=(vm, vm, vm),
            scratch_shapes=[
                pltpu.VMEM((2, R, H), F32),
                pltpu.VMEM((T, rows, D), BF16),
                pltpu.VMEM((T, rows, H), BF16),
                pltpu.VMEM((T + 1, F, rows, R), BF16),
                pltpu.VMEM((T, F, rows, R), BF16),
                pltpu.VMEM((rows, D), F32),
                DMA((2, G)), DMA((2, T)), DMA((2, T)),
                DMA((2, Y, NC)), DMA((2, Y, NC)),
                DMA((2, Y, NC, G)), DMA((2, Y, NC, G)),
                DMA((2, Y, NC, G)), DMA((2, Y, NC, G)),
                DMA((2,)), DMA((2,)),
                DMA((T, F)), DMA((T + 1, F)),
            ],
            compiler_params=pltpu.CompilerParams(collective_id=0, has_side_effects=True,
                                                 vmem_limit_bytes=40 * 1024 * 1024),
            name="layer",
        )(prompt_tokens, pre_gain.reshape(R, 1), post_gain.reshape(1, D), up_weight, down_weight)
        whole = jax.ShapeDtypeStruct((F * R, H), BF16)
        up_o, down_o = pl.pallas_call(
            out_kernel, out_shape=(whole, whole), in_specs=[vm, vm], out_specs=(any_, any_),
            scratch_shapes=[DMA((2, 8))], name="put",
        )(up, down)
        return mixed, up_o, down_o

    placed = (P(("grp", "fs", "tp"), None), P("fs", "tp"), P("fs", "tp"), P("fs"), P())
    return jax.shard_map(
        per_device,
        mesh=mesh,
        in_specs=placed,
        out_specs=(P(("grp", "fs", "tp"), None), P("grp", "tp"), P("grp", "tp")),
        check_vma=False,
    )
```

time: 266 us -> 119 us (0.45)
  waiting for transfers between devices: 204 us -> 0 us
  Pallas kernels: 0 us -> 109 us
  matrix products: 16.5 us -> 0 us
  other arithmetic: 14.1 us -> 0 us
  between operations: 13.8 us -> 0.66 us
  local copies, waits for them, and re-layouts: 16.9 us -> 8.76 us
    all_gather x3 -> x0, waiting for transfers between devices: 160 us -> none  [the longest x1 60.4 us: per_device(): lax.all_gather(down_local, 'fs', axis=0, tiled=True)]
    pallas_call x0 -> x2, Pallas kernels: none -> 109 us  [the longest x1 97.4 us: per_device(): pl.pallas_call(functools.partial(layer_kernel, (G, F, T, NC)), out_shape=...]
    reduce_scatter x1 -> x0, waiting for transfers between devices: 43.8 us -> none  [per_device(): lax.psum_scatter(lax.dot_general(hidden, sampler_down, (((1,), (1,)), (()...]
    dot_general x1 -> x0, matrix products: 16.5 us -> none  [per_device(): lax.dot_general(hidden, sampler_down, (((1,), (1,)), ((), ())), preferred...]
    convert_element_type x4 -> x0, other arithmetic: 11.6 us -> none  [the longest x1 3.83 us: per_device(): down_local = down_weight.astype(jnp.bfloat16)]
    unnamed x4 -> x7, local copies, waits for them, and re-layouts: 16.9 us -> 7.23 us
  transfers between devices with their start and end apart: 4 -> 0, of which waited for: 4 -> 0; matrix products, arithmetic and copies ran while one was open for 3% -> 0% of each run, Pallas kernels for 0% -> 0%
where the time goes in v1:
time: 119 us
  Pallas kernels  109 us (92%)
  local copies, waits for them, and re-layouts  8.76 us (7%)
    pallas_call x1, Pallas kernels, per_device(): pl.pallas_call(functools.partial(layer_kernel, (G, F, T, NC)), out_shape=...  97.4 us
    pallas_call x1, Pallas kernels, per_device(): pl.pallas_call(out_kernel, out_shape=(whole, whole), in_specs=[vm, vm], o...  11.8 us
    unnamed x7, local copies, waits for them, and re-layouts  7.23 us

profile of v1, /device:TPU:0, one launch (start us, length us, event | category | flops | bytes accessed | tf_op | source)
XLA Modules:
  0.0 118.6 jit_solution(10487794531058166584)
XLA Ops:
  0.6 1.5 %copy.8.gain_ref = f32[512,1]{1,0:T(8,128)} copy(f32[512,1]{0,1:T(1,128)} %bitcast.3) | data formatting | bytes 4096 | tf_op jit(solution)/shard_map/reshape | solution.py:352
  2.2 97.4 %layer.1 = (bf16[128,2048]{1,0:T(8,128)(2,1)}, bf16[2048,2048]{1,0:T(8,128)(2,1)S(1)}, bf16[2048,2048]{1,0:T(8,128)(2,1)S(1)}) custom-call(bf16[128,2048]{1,0:T(8,128)(2,1)} %tok_ref.1, f32[512,1]{1,0:T(8,128)} %copy.8.gain_ref, f32[1,2048]{1,0:T(1,128)} %bitcast.2, f32[512,2048]{1,0:T(8,128)} %up_hbm.1, f32[512,2048]{1,0:T(8,128)} %down_hbm.1), custom_call_target="tpu_custom_call" | custom-call | tf_op jit(solution)/shard_map/layer/pallas_call | solution.py:329
  99.6 0.0 copy-start
  99.6 3.2 %copy-done = bf16[2048,2048]{1,0:T(8,128)(2,1)} copy-done((bf16[2048,2048]{1,0:T(8,128)(2,1)}, bf16[2048,2048]{1,0:T(8,128)(2,1)S(1)}, u32[]{:S(2)}) %copy-start) | copy-done | bytes 8388632
  102.8 0.0 copy-start.1
  102.8 3.2 %copy-done.1 = bf16[2048,2048]{1,0:T(8,128)(2,1)} copy-done((bf16[2048,2048]{1,0:T(8,128)(2,1)}, bf16[2048,2048]{1,0:T(8,128)(2,1)S(1)}, u32[]{:S(2)}) %copy-start.1) | copy-done | bytes 8388632
  106.0 0.0 copy-start.2
  106.0 11.8 %put.1 = (bf16[2048,2048]{1,0:T(8,128)(2,1)}, bf16[2048,2048]{1,0:T(8,128)(2,1)}) custom-call(bf16[2048,2048]{1,0:T(8,128)(2,1)} %copy-done, bf16[2048,2048]{1,0:T(8,128)(2,1)} %copy-done.1), custom_call_target="tpu_custom_call" | custom-call | tf_op jit(solution)/shard_map/put/pallas_call | solution.py:354
  117.8 0.0 copy-done.2
  117.8 0.8 copy.10
Async XLA Ops:
  99.6 3.2 %copy-start = (bf16[2048,2048]{1,0:T(8,128)(2,1)}, bf16[2048,2048]{1,0:T(8,128)(2,1)S(1)}, u32[]{:S(2)}) copy-start(bf16[2048,2048]{1,0:T(8,128)(2,1)S(1)} %get-tuple-element.9.up_v) | copy-start | bytes 25165828
  102.8 3.2 %copy-start.1 = (bf16[2048,2048]{1,0:T(8,128)(2,1)}, bf16[2048,2048]{1,0:T(8,128)(2,1)S(1)}, u32[]{:S(2)}) copy-start(bf16[2048,2048]{1,0:T(8,128)(2,1)S(1)} %get-tuple-element.10.down_v) | copy-start | bytes 25165828
  106.0 11.8 %copy-start.2 = (bf16[128,2048]{1,0:T(8,128)(2,1)S(1)}, bf16[128,2048]{1,0:T(8,128)(2,1)}, u32[]{:S(2)}) copy-start(bf16[128,2048]{1,0:T(8,128)(2,1)} %get-tuple-element.16) | copy-start | bytes 1572868

commit v2 on v1

--- a/solution.py
+++ b/solution.py
@@ -8,13 +8,14 @@
 from jax.sharding import PartitionSpec as P
 
 MESH = pl.DeviceIdType.MESH
+S = 2
 BF16 = jnp.bfloat16
 F32 = jnp.float32
 
 
 def layer_kernel(sizes, tok_ref, gain_ref, post_ref, up_hbm, down_hbm, mixed_ref, up_full, down_full,
-                 stage, tok, hidden, rbuf, sbuf, total,
-                 load_sem, tsend, trecv, ysend, yrecv, xsend, xrecv, csend, crecv, osend, orecv, rsend, rrecv):
+                 stage, gain_cols, tok, hidden, rbuf, sbuf, total,
+                 first_sem, load_sem, tsend, trecv, ysend, yrecv, xsend, xrecv, csend, crecv, osend, orecv, rsend, rrecv):
     G, F, T, NC = sizes
     Y = F // 2
     g, fs, z = lax.axis_index("grp"), lax.axis_index("fs"), lax.axis_index("tp")
@@ -32,9 +33,14 @@
         r = pl.ds(pl.multiple_of(((g + e) % G) * piece, piece), piece)
         return pltpu.make_async_copy(hbm[m].at[r], stage.at[m, r], load_sem.at[m, e])
 
-    for m in range(2):
-        for e in range(G):
-            loads(m, e).start()
+    def first_load(q):
+        r = pl.ds(pl.multiple_of(g * piece + q * CR, CR), CR)
+        return pltpu.make_async_copy(up_hbm.at[r], stage.at[0, r], first_sem.at[q])
+
+    for q in range(NC):
+        first_load(q).start()
+    for m, e in [(1, 0)] + [(m, e) for m in range(2) for e in range(1, G)]:
+        loads(m, e).start()
 
     barrier = pltpu.get_barrier_semaphore()
     for d in range(1, Y):
@@ -51,6 +57,10 @@
     def _():
         pl.semaphore_signal(barrier, inc=1, device_id={"tp": z + 1}, device_id_type=MESH)
 
+    L = gain_cols.shape[1]
+    for i in range(0, R, L):
+        gain_cols[i:i + L, :] = jnp.transpose(jnp.broadcast_to(gain_ref[:, i:i + L], (L, L)))
+
     values = tok_ref[...].astype(F32)
     scale = lax.rsqrt(jnp.mean(values * values, axis=1, keepdims=True) + 1e-06)
     tok[z] = (values * scale).astype(BF16)
@@ -60,7 +70,7 @@
             r = pl.ds(pl.multiple_of(start + i, CR), CR)
             v = stage[m, r, :]
             if m == 0:
-                v = v * gain_ref[r, :]
+                v = v * gain_cols[r, 0:1]
             full[m][pl.ds(pl.multiple_of(fs * R + start + i, CR), CR), :] = v.astype(BF16)
 
     def remote(ref, rows, ss, rs, dev):
@@ -104,17 +114,17 @@
 
     pl.semaphore_wait(barrier, (Y - 1) + (G - 1) + 1 + not_first.astype(jnp.int32) + not_last.astype(jnp.int32))
 
-    def tok_out(dirn, k):
-        b = z - k if dirn == 0 else z + k
+    def tok_move(dirn, k, p, b):
         dev = z + 1 if dirn == 0 else z - 1
-        return pltpu.make_async_remote_copy(tok.at[b], tok.at[b], tsend.at[dirn, k], trecv.at[dirn, k],
+        r = pl.ds(p * (rows_t // S), rows_t // S)
+        return pltpu.make_async_remote_copy(tok.at[b, r], tok.at[b, r], tsend.at[dirn, k, p], trecv.at[dirn, k, p],
                                             device_id={"tp": dev}, device_id_type=MESH)
 
-    def tok_in(dirn, k):
-        b = z - k - 1 if dirn == 0 else z + k + 1
-        dev = z + 1 if dirn == 0 else z - 1
-        return pltpu.make_async_remote_copy(tok.at[b], tok.at[b], tsend.at[dirn, k], trecv.at[dirn, k],
-                                            device_id={"tp": dev}, device_id_type=MESH)
+    def tok_out(dirn, k, p):
+        return tok_move(dirn, k, p, z - k if dirn == 0 else z + k)
+
+    def tok_in(dirn, k, p):
+        return tok_move(dirn, k, p, z - k - 1 if dirn == 0 else z + k + 1)
 
     def has_out(dirn, k):
         return (z - k >= 0) & not_last if dirn == 0 else (z + k <= T - 1) & not_first
@@ -122,22 +132,26 @@
     def has_in(dirn, k):
         return z - k - 1 >= 0 if dirn == 0 else z + k + 1 <= T - 1
 
-    def tok_step(k):
+    def tok_step(k, p):
         for dirn in range(2):
             if k > 0:
                 @pl.when(has_in(dirn, k - 1))
                 def _():
-                    tok_in(dirn, k - 1).wait_recv()
+                    tok_in(dirn, k - 1, p).wait_recv()
             if k < T - 1:
                 @pl.when(has_out(dirn, k))
                 def _():
-                    tok_out(dirn, k).start()
-
-    tok_step(0)
+                    tok_out(dirn, k, p).start()
+
+    for p in range(S):
+        tok_step(0, p)
 
     for m in range(2):
-        loads(m, 0).wait()
+        if m:
+            loads(m, 0).wait()
         for q in range(NC):
+            if not m:
+                first_load(q).wait()
             convert(m, pl.multiple_of(g * piece, piece) + q * CR, CR)
             for d in range(1, Y):
                 y_copy(m, d, q).start()
@@ -160,14 +174,13 @@
 
     LAG = 2
     steps = NC + LAG
-    tok_at = {max(1, (steps * k) // (T - 1)): k for k in range(1, T - 1)}
+    tok_steps = [(k, p) for k in range(1, T - 1) for p in range(S)]
     for q in range(steps):
         fwd(0, q)
-        if q in tok_at:
-            tok_step(tok_at[q])
-    for k in range(1, T - 1):
-        if k not in tok_at.values():
-            tok_step(k)
+        if q % 2 == 1 and tok_steps:
+            tok_step(*tok_steps.pop(0))
+    for k, p in tok_steps:
+        tok_step(k, p)
     own_copy(0, False).wait_recv()
     for d in range(1, Y):
         for q in range(NC):
@@ -188,13 +201,17 @@
         w = down_full[pl.ds(pl.multiple_of(f * R, R), R), :]
         return lax.dot_general(hidden[t], w, (((1,), (1,)), ((), ())), preferred_element_type=F32).astype(BF16)
 
-    side = jnp.minimum(z, T - 1 - z)
-
-    def order(k):
-        n = T - 1 - k
-        near = jnp.where(n % 2 == 1, z + (n + 1) // 2, z - n // 2)
-        far = jnp.where(z < T - 1 - z, z + (n - side), z - (n - side))
-        return jnp.where(n <= 2 * side, near, far)
+    lower = 2 * z < T
+
+    def near(k):
+        up = jnp.where(k < T - 1 - z, z + 1 + k, T - 2 - k)
+        down = jnp.where(k < z, z - 1 - k, k + 1)
+        return jnp.where(lower, up, down)
+
+    def far(k):
+        up = jnp.where(k < T - 1 - z, T - 1 - k, k - (T - 1 - z))
+        down = jnp.where(k < z, k, T - 1 - (k - z))
+        return jnp.where(lower, up, down)
 
     def rs_copy(t, f, right):
         dev = z + 1 if right else z - 1
@@ -206,26 +223,31 @@
         return pltpu.make_async_remote_copy(sbuf.at[0, f], rbuf.at[slot, f], rsend.at[0, f], rrecv.at[slot, f],
                                             device_id={"tp": z}, device_id_type=MESH)
 
+    def is_inner(t):
+        return ((t > z) & not_first) | ((t < z) & not_last)
+
+    def rs_start(t, f):
+        @pl.when(t > z)
+        def _():
+            rs_copy(t, f, True).start()
+
+        @pl.when(t < z)
+        def _():
+            rs_copy(t, f, False).start()
+
     def unit(t, f):
-        p = second_mm(t, f)
-        inner = ((t > z) & not_first) | ((t < z) & not_last)
-
-        @pl.when(inner)
+        sbuf[t, f] = second_mm(t, f)
+
+        @pl.when(jnp.logical_not(is_inner(t)))
+        def _():
+            rs_start(t, f)
+
+    def merge(t, f):
+        @pl.when(is_inner(t))
         def _():
             rs_in(t, f).wait_recv()
-            sbuf[t, f] = (p.astype(F32) + rbuf[t, f].astype(F32)).astype(BF16)
-
-        @pl.when(jnp.logical_not(inner))
-        def _():
-            sbuf[t, f] = p
-
-        @pl.when(t > z)
-        def _():
-            rs_copy(t, f, True).start()
-
-        @pl.when(t < z)
-        def _():
-            rs_copy(t, f, False).start()
+            sbuf[t, f] = (sbuf[t, f].astype(F32) + rbuf[t, f].astype(F32)).astype(BF16)
+            rs_start(t, f)
 
     def feature(d, other):
         return ((y - d + Y) % Y) * 2 + (1 - c if other else c)
@@ -243,28 +265,35 @@
                 fwd(1, todo.pop(0))
 
     for k in range(T):
-        t = order(k) if k < T - 1 else z
-        if k == 0:
-            tok_step(T - 1)
+        t = near(k) if k < T - 1 else z
+        if k == T - 2:
+            for p in range(S):
+                tok_step(T - 1, p)
         first_mm(t)
-        some(1)
         for other in range(2):
             if k < T - 1:
                 unit(t, feature(0, other))
+                some(1)
             else:
                 own_unit(feature(0, other))
+    for k in range(T - 1):
+        for other in range(2):
+            merge(near(k), feature(0, other))
             some(1)
     some(len(todo))
     for d in range(1, Y):
         for q in range(NC):
             for e in range(G):
                 c_in(1, d, q, e).wait_recv()
-    for d in range(1, Y):
-        for other in range(2):
-            f = feature(d, other)
-            for k in range(T - 1):
-                unit(order(k), f)
-            own_unit(f)
+    rest = [feature(d, other) for d in range(1, Y) for other in range(2)]
+    for k in range(T - 1):
+        for f in rest:
+            unit(far(k), f)
+    for f in rest:
+        own_unit(f)
+    for k in range(T - 1):
+        for f in rest:
+            merge(far(k), f)
 
     for f in range(F):
         cols = pl.ds(f * R, R)
@@ -287,7 +316,7 @@
         for dirn in range(2):
             @pl.when(has_out(dirn, k))
             def _():
-                tok_out(dirn, k).wait_send()
+                [tok_out(dirn, k, p).wait_send() for p in range(S)]
     for m in range(2):
         own_copy(m, True).wait_send()
         for d in range(1, Y):
@@ -298,20 +327,9 @@
                         x_copy(m, d, q, e).wait_send()
                     c_copy(m, d, q, e).wait_send()
     for k in range(T - 1):
-        t = order(k)
+        t = near(k)
         for f in range(F):
             rs_copy(t, f, True).wait_send()
-
-
-def out_kernel(up_v, down_v, up_o, down_o, sem):
-    n = sem.shape[1]
-    r = up_v.shape[0] // n
-    cps = [pltpu.make_async_copy(a.at[pl.ds(i * r, r)], b.at[pl.ds(i * r, r)], sem.at[m, i])
-           for m, (a, b) in enumerate(((up_v, up_o), (down_v, down_o))) for i in range(n)]
-    for cp in cps:
-        cp.start()
-    for cp in cps:
-        cp.wait()
 
 
 def solution(mesh):
@@ -324,6 +342,7 @@
         piece = R // G
         CR = max(16, piece // 8)
         NC = piece // CR
+        L = min(128, R)
         DMA = pltpu.SemaphoreType.DMA
         vm, any_ = pl.BlockSpec(memory_space=pltpu.VMEM), pl.BlockSpec(memory_space=pl.ANY)
         mixed, up, down = pl.pallas_call(
@@ -334,12 +353,13 @@
             out_specs=(vm, vm, vm),
             scratch_shapes=[
                 pltpu.VMEM((2, R, H), F32),
+                pltpu.VMEM((R, L), F32),
                 pltpu.VMEM((T, rows, D), BF16),
                 pltpu.VMEM((T, rows, H), BF16),
                 pltpu.VMEM((T + 1, F, rows, R), BF16),
                 pltpu.VMEM((T, F, rows, R), BF16),
                 pltpu.VMEM((rows, D), F32),
-                DMA((2, G)), DMA((2, T)), DMA((2, T)),
+                DMA((NC,)), DMA((2, G)), DMA((2, T, S)), DMA((2, T, S)),
                 DMA((2, Y, NC)), DMA((2, Y, NC)),
                 DMA((2, Y, NC, G)), DMA((2, Y, NC, G)),
                 DMA((2, Y, NC, G)), DMA((2, Y, NC, G)),
@@ -349,13 +369,8 @@
             compiler_params=pltpu.CompilerParams(collective_id=0, has_side_effects=True,
                                                  vmem_limit_bytes=40 * 1024 * 1024),
             name="layer",
-        )(prompt_tokens, pre_gain.reshape(R, 1), post_gain.reshape(1, D), up_weight, down_weight)
-        whole = jax.ShapeDtypeStruct((F * R, H), BF16)
-        up_o, down_o = pl.pallas_call(
-            out_kernel, out_shape=(whole, whole), in_specs=[vm, vm], out_specs=(any_, any_),
-            scratch_shapes=[DMA((2, 8))], name="put",
-        )(up, down)
-        return mixed, up_o, down_o
+        )(prompt_tokens, pre_gain.reshape(1, R), post_gain.reshape(1, D), up_weight, down_weight)
+        return mixed, up, down
 
     placed = (P(("grp", "fs", "tp"), None), P("fs", "tp"), P("fs", "tp"), P("fs"), P())
     return jax.shard_map(

time: 119 us -> 99.7 us (0.84)
  Pallas kernels: 109 us -> 91.3 us
    pallas_call x1 -> x0, Pallas kernels: 11.8 us -> none  [per_device(): pl.pallas_call(out_kernel, out_shape=(whole, whole), in_specs=[vm, vm], o...]
    pallas_call x1, Pallas kernels: 97.4 us -> 91.3 us  [per_device(): pl.pallas_call(functools.partial(layer_kernel, (G, F, T, NC)), out_shape=...]
    reshape x1 -> x0, local copies, waits for them, and re-layouts: 1.53 us -> none  [per_device(): pre_gain.reshape(R, 1)]
    unnamed x7 -> x5, local copies, waits for them, and re-layouts: 7.23 us -> 7.59 us
where the time goes in v2:
time: 99.7 us; the launch traced here: 99.5 us
  Pallas kernels  91.3 us (92%)
  local copies, waits for them, and re-layouts  7.59 us (8%)
    pallas_call x1, Pallas kernels, per_device(): pl.pallas_call(functools.partial(layer_kernel, (G, F, T, NC)), out_shape=...  91.3 us
    unnamed x5, local copies, waits for them, and re-layouts  7.59 us

profile of v2, /device:TPU:0, one launch (start us, length us, event | category | flops | bytes accessed | tf_op | source)
XLA Modules:
  0.0 99.5 jit_solution(10481323291782247156)
XLA Ops:
  0.6 91.3 %layer.1 = (bf16[128,2048]{1,0:T(8,128)(2,1)}, bf16[2048,2048]{1,0:T(8,128)(2,1)S(1)}, bf16[2048,2048]{1,0:T(8,128)(2,1)S(1)}) custom-call(bf16[128,2048]{1,0:T(8,128)(2,1)} %tok_ref.1, f32[1,512]{1,0:T(1,128)} %bitcast.3, f32[1,2048]{1,0:T(1,128)} %bitcast.2, f32[512,2048]{1,0:T(8,128)} %up_hbm.1, f32[512,2048]{1,0:T(8,128)} %down_hbm.1), custom_call_target="tpu_custom_call" | custom-call | tf_op jit(solution)/shard_map/layer/pallas_call | solution.py:348
  91.9 3.4 %copy.11 = bf16[2048,2048]{1,0:T(8,128)(2,1)} copy(bf16[2048,2048]{1,0:T(8,128)(2,1)S(1)} %get-tuple-element.4) | data formatting | bytes 16777216
  95.3 0.0 copy-start
  95.3 3.4 %copy.12 = bf16[2048,2048]{1,0:T(8,128)(2,1)} copy(bf16[2048,2048]{1,0:T(8,128)(2,1)S(1)} %get-tuple-element.5) | data formatting | bytes 16777216
  98.7 0.0 copy-done
  98.7 0.8 copy.13
Async XLA Ops:
  95.3 3.4 %copy-start = (bf16[128,2048]{1,0:T(8,128)(2,1)S(1)}, bf16[128,2048]{1,0:T(8,128)(2,1)}, u32[]{:S(2)}) copy-start(bf16[128,2048]{1,0:T(8,128)(2,1)} %get-tuple-element.9) | copy-start | bytes 1572868

commit v3 on v2

--- a/solution.py
+++ b/solution.py
@@ -174,10 +174,11 @@
 
     LAG = 2
     steps = NC + LAG
+    TOK_GAP = max(2, NC // 4)
     tok_steps = [(k, p) for k in range(1, T - 1) for p in range(S)]
     for q in range(steps):
         fwd(0, q)
-        if q % 2 == 1 and tok_steps:
+        if q % TOK_GAP == TOK_GAP - 1 and tok_steps:
             tok_step(*tok_steps.pop(0))
     for k, p in tok_steps:
         tok_step(k, p)
@@ -273,13 +274,13 @@
         for other in range(2):
             if k < T - 1:
                 unit(t, feature(0, other))
-                some(1)
+                some(-(-steps // 12))
             else:
                 own_unit(feature(0, other))
     for k in range(T - 1):
         for other in range(2):
             merge(near(k), feature(0, other))
-            some(1)
+            some(-(-steps // 12))
     some(len(todo))
     for d in range(1, Y):
         for q in range(NC):
@@ -340,7 +341,7 @@
         rows, D = prompt_tokens.shape
         R, H = up_weight.shape
         piece = R // G
-        CR = max(16, piece // 8)
+        CR = max(16, piece // 16)
         NC = piece // CR
         L = min(128, R)
         DMA = pltpu.SemaphoreType.DMA

time: 99.7 us -> 109 us (1.093)
  Pallas kernels: 91.3 us -> 101 us
    pallas_call x1, Pallas kernels: 91.3 us -> 101 us  [per_device(): pl.pallas_call(functools.partial(layer_kernel, (G, F, T, NC)), out_shape=...]
where the time goes in v3:
time: 109 us
  Pallas kernels  101 us (93%)
  local copies, waits for them, and re-layouts  7.59 us (7%)
    pallas_call x1, Pallas kernels, per_device(): pl.pallas_call(functools.partial(layer_kernel, (G, F, T, NC)), out_shape=...  101 us
    unnamed x5, local copies, waits for them, and re-layouts  7.59 us

profile of v3, /device:TPU:0, one launch (start us, length us, event | category | flops | bytes accessed | tf_op | source)
XLA Modules:
  0.0 109.1 jit_solution(17532758504217886992)
XLA Ops:
  0.6 100.8 %layer.1 = (bf16[128,2048]{1,0:T(8,128)(2,1)}, bf16[2048,2048]{1,0:T(8,128)(2,1)S(1)}, bf16[2048,2048]{1,0:T(8,128)(2,1)S(1)}) custom-call(bf16[128,2048]{1,0:T(8,128)(2,1)} %tok_ref.1, f32[1,512]{1,0:T(1,128)} %bitcast.3, f32[1,2048]{1,0:T(1,128)} %bitcast.2, f32[512,2048]{1,0:T(8,128)} %up_hbm.1, f32[512,2048]{1,0:T(8,128)} %down_hbm.1), custom_call_target="tpu_custom_call" | custom-call | tf_op jit(solution)/shard_map/layer/pallas_call | solution.py:349
  101.5 3.4 %copy.11 = bf16[2048,2048]{1,0:T(8,128)(2,1)} copy(bf16[2048,2048]{1,0:T(8,128)(2,1)S(1)} %get-tuple-element.4) | data formatting | bytes 16777216
  104.9 0.0 copy-start
  104.9 3.4 %copy.12 = bf16[2048,2048]{1,0:T(8,128)(2,1)} copy(bf16[2048,2048]{1,0:T(8,128)(2,1)S(1)} %get-tuple-element.5) | data formatting | bytes 16777216
  108.3 0.0 copy-done
  108.3 0.8 copy.13
Async XLA Ops:
  104.9 3.4 %copy-start = (bf16[128,2048]{1,0:T(8,128)(2,1)S(1)}, bf16[128,2048]{1,0:T(8,128)(2,1)}, u32[]{:S(2)}) copy-start(bf16[128,2048]{1,0:T(8,128)(2,1)} %get-tuple-element.9) | copy-start | bytes 1572868
